TPU v7x, 128 devices: a whole 4x4x4 slice. The times are simulated.
128 devices in a mesh: sp: 16 (over z, y), tp: 8 (over x, core).
Axes of the slice: x: 4, y: 4, z: 4, core: 2. Of those that a mesh axis runs over, the one named last changes fastest.
Arguments:
- hidden: bfloat16 [16, 1024, 1024], P(None, 'sp'), may hold values from -0.09375 to 0.09375
- value_weight: bfloat16 [1024, 1024], P(None, 'tp'), may hold values from -0.75 to 0.75
- queries: bfloat16 [16, 8, 1024, 64], P(None, 'tp', 'sp'), may hold values from -0.1875 to 0.1875
- key_vectors: bfloat16 [16, 8, 1024, 64], P(None, 'tp', 'sp'), may hold values from -0.1875 to 0.1875
- forward_decay: float32 [16, 8, 1024, 64], P(None, 'tp', 'sp'), may hold values from -0.0029296875 to -9.765625e-06
- backward_decay: float32 [16, 8, 1024, 64], P(None, 'tp', 'sp'), may hold values from -0.0029296875 to -9.765625e-06
- cotangent: bfloat16 [16, 1024, 1024], P(None, 'sp', 'tp'), may hold values from -6 to 6
Outputs:
- grad_queries: bfloat16 [16, 8, 1024, 64], P(None, 'tp', 'sp')
- grad_keys: bfloat16 [16, 8, 1024, 64], P(None, 'tp', 'sp')
- grad_forward: float32 [16, 8, 1024, 64], P(None, 'tp', 'sp')
- grad_backward: float32 [16, 8, 1024, 64], P(None, 'tp', 'sp')
- grad_hidden: bfloat16 [16, 1024, 1024], P(None, 'sp', 'tp')
- grad_weight: float32 [1024, 1024], P('sp', 'tp')
All inputs are finite; a program needn't handle non-finite values.
Results may differ from a plain program's by a relative error of at most 0.015.
Values may be sent and summed in bfloat16 or wider, within the bound.
A program may use at most 128 MiB of HBM per device.

v0:
```python
import jax
import jax.numpy as jnp
from jax import lax
from jax.sharding import Mesh
from jax.sharding import PartitionSpec as P

SP = ("sp_0", "sp_1")


EXACT_DOTS = lax.Precision.HIGHEST


def nothing_yet(x, identity):
    return jax.tree.map(
        lambda part, zero: jnp.zeros_like(part) + jnp.asarray(zero, part.dtype), x, identity
    )


def prefix_by_axis(x, axes, combine, identity, reverse):
    before = start = nothing_yet(x, identity)
    running = x
    for axis in reversed(axes):
        length, index = lax.axis_size(axis), lax.axis_index(axis)
        pieces = jax.tree.map(lambda part: lax.all_gather(part, axis), running)
        inside, running = start, start
        for k in reversed(range(length)) if reverse else range(length):
            passed = k > index if reverse else k < index
            running = combine(running, jax.tree.map(lambda part: part[k], pieces))
            inside = jax.tree.map(lambda new, old: jnp.where(passed, new, old), running, inside)
        before = combine(inside, before)
    return before


def own_rows(running, axes):
    for axis in axes:
        running = lax.psum_scatter(running, axis, scatter_dimension=0, tiled=True)
    return running


def flip_tokens(tensor, axis_number):
    return jnp.flip(tensor, axis=axis_number)


def elements(query_heads, key_heads, value_heads, decay_heads, seed_heads):
    cumulative = jnp.cumsum(decay_heads, axis=2)
    final_sum = cumulative[:, :, -1, :]
    to_end = jnp.exp(final_sum[:, :, None, :] - cumulative)
    factor = jnp.exp(final_sum)
    state_part = jnp.einsum(
        "bhjd,bhje->bhde", key_heads * to_end, value_heads, precision=EXACT_DOTS
    )
    grad_part = jnp.einsum(
        "bhcd,bhce->bhde", query_heads * jnp.exp(cumulative), seed_heads, precision=EXACT_DOTS
    )
    return ((factor, state_part), (factor, grad_part))


def compose(earlier, later):
    return (earlier[0] * later[0], later[0][..., None] * earlier[1] + later[1])


def neutral(element):
    return (jnp.ones_like(element[0]), jnp.zeros_like(element[1]))


def paired(first, second):
    return (jnp.stack([first[0], second[0]]), jnp.stack([first[1], second[1]]))


def block_grads(query_seq, key_seq, value_seq, decay_seq, seed_seq, state_in, grad_in):
    length = query_seq.shape[1]
    seed_real = seed_seq.astype(jnp.float32)
    value_real = value_seq.astype(jnp.float32)
    cumulative = jnp.cumsum(decay_seq, axis=1)
    final_sum = cumulative[:, -1, :]
    growth = jnp.exp(cumulative)
    shrink = jnp.exp(-cumulative)
    to_end = jnp.exp(final_sum[:, None, :] - cumulative)
    query_hat = (query_seq * growth).astype(jnp.bfloat16)
    key_hat = (key_seq * shrink).astype(jnp.bfloat16)
    below_mask = jnp.tril(jnp.ones((length, length), dtype=bool))[None]
    scores = jnp.where(
        below_mask,
        jnp.einsum("hid,hjd->hij", query_hat, key_hat, preferred_element_type=jnp.float32),
        0.0,
    ).astype(jnp.bfloat16)
    seed_scores = jnp.where(
        below_mask,
        jnp.einsum("hie,hje->hij", seed_seq, value_seq, preferred_element_type=jnp.float32),
        0.0,
    ).astype(jnp.bfloat16)
    grad_query = growth * (
        jnp.einsum("hij,hjd->hid", seed_scores, key_hat, preferred_element_type=jnp.float32)
        + jnp.einsum("hce,hde->hcd", seed_real, state_in, precision=EXACT_DOTS)
    )
    grad_key = shrink * jnp.einsum(
        "hij,hid->hjd", seed_scores, query_hat, preferred_element_type=jnp.float32
    )
    grad_key = grad_key + to_end * jnp.einsum(
        "hde,hje->hjd", grad_in, value_real, precision=EXACT_DOTS
    )
    grad_value = jnp.einsum("hij,hie->hje", scores, seed_seq, preferred_element_type=jnp.float32)
    grad_value = grad_value + jnp.einsum(
        "hjd,hde->hje", key_seq * to_end, grad_in, precision=EXACT_DOTS
    )
    grad_cumul = query_seq * grad_query - key_seq * grad_key
    return (grad_query, grad_key, grad_value, grad_cumul)


def per_device(
    hidden, value_weight, queries, key_vectors, forward_decay, backward_decay, cotangent
):
    batch_size, length, model_width = hidden.shape
    head_count = queries.shape[1]
    value_width = value_weight.shape[1] // head_count
    hidden_rows = hidden.reshape(batch_size * length, model_width)
    values_flat = jnp.dot(hidden_rows, value_weight, preferred_element_type=jnp.float32).astype(
        jnp.bfloat16
    )

    def to_heads(tensor):
        return tensor.reshape(batch_size, length, head_count, value_width).transpose(0, 2, 1, 3)

    value_narrow = to_heads(values_flat)
    seed_narrow = to_heads(cotangent)
    value_heads = value_narrow.astype(jnp.float32)
    seed_heads = seed_narrow.astype(jnp.float32)
    query_heads = queries.astype(jnp.float32)
    key_heads = key_vectors.astype(jnp.float32)
    ahead_state, ahead_grad = elements(
        query_heads, key_heads, value_heads, forward_decay, seed_heads
    )
    behind_state, behind_grad = elements(
        flip_tokens(query_heads, 2),
        flip_tokens(key_heads, 2),
        flip_tokens(value_heads, 2),
        flip_tokens(backward_decay, 2),
        flip_tokens(seed_heads, 2),
    )
    lower_pair = paired(ahead_state, behind_grad)
    upper_pair = paired(behind_state, ahead_grad)
    from_lower = prefix_by_axis(lower_pair, SP, compose, neutral(lower_pair), False)[1]
    from_higher = prefix_by_axis(upper_pair, SP, compose, neutral(upper_pair), True)[1]
    state_left, grad_left = (from_lower[0], from_lower[1])
    state_right, grad_right = (from_higher[0], from_higher[1])

    def per_sequence(inputs):
        (
            query_seq,
            key_seq,
            value_seq,
            ahead_decay,
            behind_decay,
            seed_seq,
            left_state,
            right_grad,
            right_state,
            left_grad,
        ) = inputs
        ahead = block_grads(
            query_seq, key_seq, value_seq, ahead_decay, seed_seq, left_state, right_grad
        )
        behind = block_grads(
            flip_tokens(query_seq, 1),
            flip_tokens(key_seq, 1),
            flip_tokens(value_seq, 1),
            flip_tokens(behind_decay, 1),
            flip_tokens(seed_seq, 1),
            right_state,
            left_grad,
        )
        return (
            ahead[0] + flip_tokens(behind[0], 1),
            ahead[1] + flip_tokens(behind[1], 1),
            ahead[2] + flip_tokens(behind[2], 1),
            ahead[3],
            flip_tokens(behind[3], 1),
        )

    grad_query, grad_key, grad_value, cumul_ahead, cumul_behind = lax.map(
        per_sequence,
        (
            query_heads,
            key_heads,
            value_narrow,
            forward_decay,
            backward_decay,
            seed_narrow,
            state_left,
            grad_right,
            state_right,
            grad_left,
        ),
    )
    totals = jnp.stack([jnp.sum(cumul_ahead, axis=2), jnp.sum(cumul_behind, axis=2)])
    before = prefix_by_axis(
        totals, SP, lambda earlier, later: earlier + later, jnp.zeros_like(totals), False
    )
    grad_forward = -(before[0][:, :, None, :] + jnp.cumsum(cumul_ahead, axis=2) - cumul_ahead)
    grad_backward = before[1][:, :, None, :] + jnp.cumsum(cumul_behind, axis=2)
    value_rows = (
        grad_value.transpose(0, 2, 1, 3)
        .reshape(batch_size * length, head_count * value_width)
        .astype(jnp.bfloat16)
    )

    def weight_term(row_count):
        columns = lax.slice_in_dim(hidden_rows, 0, row_count, axis=1)
        return lax.dot_general(
            columns, value_rows, (((0,), (0,)), ((), ())), preferred_element_type=jnp.float32
        )

    grad_weight = own_rows(weight_term(model_width // lax.axis_size(SP) * lax.axis_size(SP)), SP)
    input_terms = lax.dot_general(
        value_rows, value_weight, (((1,), (1,)), ((), ())), preferred_element_type=jnp.float32
    ).reshape(batch_size, length, model_width)
    grad_hidden = (
        lax.psum_scatter(input_terms.astype(jnp.bfloat16), "tp", scatter_dimension=2, tiled=True)
        .astype(jnp.float32)
        .astype(jnp.bfloat16)
    )
    return (
        grad_query.astype(jnp.bfloat16),
        grad_key.astype(jnp.bfloat16),
        grad_forward,
        grad_backward,
        grad_hidden,
        grad_weight,
    )


def solution(mesh):
    split = Mesh(mesh.devices.reshape(4, 4, mesh.shape["tp"]), ("sp_0", "sp_1", "tp"))
    return jax.shard_map(
        per_device,
        mesh=split,
        in_specs=(
            P(None, SP, None),
            P(None, "tp"),
            P(None, "tp", SP, None),
            P(None, "tp", SP, None),
            P(None, "tp", SP, None),
            P(None, "tp", SP, None),
            P(None, SP, "tp"),
        ),
        out_specs=(
            P(None, "tp", SP, None),
            P(None, "tp", SP, None),
            P(None, "tp", SP, None),
            P(None, "tp", SP, None),
            P(None, SP, "tp"),
            P(SP, "tp"),
        ),
        check_vma=False,
    )
```

profile of v0, /device:TPU:0, one launch (start us, length us, event | category | flops | bytes accessed | tf_op | source)
XLA Modules:
  0.0 497.9 jit_solution(11999028665855159003)
XLA Ops:
  7.2 1.2 rev.39
  8.8 1.4 fusion.120
  10.2 1.8 convolution_convert_fusion.1
  12.9 1.4 copy_convert_fusion
  14.4 2.7 multiply_bitcast_fusion
  19.8 1.2 maximum_bitcast_fusion.1
  21.9 1.7 convolution_bitcast_fusion.2
  23.6 2.1 convolution_bitcast_fusion.4
  26.9 12.7 %all-gather.2 = f32[8,16,1,64]{3,1,2,0:T(8,128)S(1)} all-gather(f32[2,16,1,64]{3,1,2,0:T(8,128)S(1)} %get-tuple-element.217), channel_id=4, replica_groups=mesh['sp_0'=4,'sp_1'=4,'tp'=8] {'sp_1'}, dimensions={0}, use_global_device_ids=true | all-gather | bytes 40960 | tf_op jit(solution)/shard_map/all_gather | solution.py:24
  39.7 32.2 %all-gather.16.cloned.1.call-done = f32[8,16,1,64,128]{4,3,2,1,0:T(8,128)} async-done(((f32[2,16,1,64,128]{4,3,2,1,0:T(8,128)}), f32[8,16,1,64,128]{4,3,2,1,0:T(8,128)}) %all-gather.16.cloned.1.call-update) | async-done | bytes 4194320 | tf_op jit(solution)/shard_map/all_gather | solution.py:24
  71.9 3.6 fusion.99
  75.5 11.9 %all-gather = f32[8,16,1,64]{3,1,2,0:T(8,128)S(1)} all-gather(f32[2,16,1,64]{3,1,2,0:T(8,128)S(1)} %get-tuple-element.218), channel_id=2, replica_groups=mesh['sp_0'=4,'sp_1'=4,'tp'=8] {'sp_1'}, dimensions={0}, use_global_device_ids=true | all-gather | bytes 40960 | tf_op jit(solution)/shard_map/all_gather | solution.py:24
  87.4 34.6 %all-gather.14.cloned.1.call-done = f32[8,16,1,64,128]{4,3,2,1,0:T(8,128)} async-done(((f32[2,16,1,64,128]{4,3,2,1,0:T(8,128)}), f32[8,16,1,64,128]{4,3,2,1,0:T(8,128)}) %all-gather.14.cloned.1.call-update) | async-done | bytes 4194320 | tf_op jit(solution)/shard_map/all_gather | solution.py:24
  122.0 3.6 fusion.107
  125.7 12.3 %all_gather.58 = f32[4,2,16,1,64]{4,2,3,1,0:T(8,128)S(1)} all-gather(f32[1,2,16,1,64]{4,2,3,1,0:T(8,128)S(1)} %get-tuple-element.202), channel_id=1, replica_groups=mesh['sp_0'=4,'sp_1'=4,'tp'=8] {'sp_0'}, dimensions={0}, use_global_device_ids=true | all-gather | bytes 40960 | tf_op jit(solution)/shard_map/all_gather | solution.py:24
  138.1 12.1 %all_gather.52 = f32[4,2,16,1,64]{4,2,3,1,0:T(8,128)S(1)} all-gather(f32[1,2,16,1,64]{4,2,3,1,0:T(8,128)S(1)} %get-tuple-element.212), channel_id=1, replica_groups=mesh['sp_0'=4,'sp_1'=4,'tp'=8] {'sp_0'}, dimensions={0}, use_global_device_ids=true | all-gather | bytes 40960 | tf_op jit(solution)/shard_map/all_gather | solution.py:24
  150.2 22.7 %all-gather.12.cloned.1.call-done = f32[4,2,16,1,64,128]{5,4,3,2,1,0:T(8,128)} async-done(((f32[1,2,16,1,64,128]{5,4,3,2,1,0:T(8,128)}), f32[4,2,16,1,64,128]{5,4,3,2,1,0:T(8,128)}) %all-gather.12.cloned.1.call-update) | async-done | bytes 4194320 | tf_op jit(solution)/shard_map/all_gather | solution.py:24
  172.9 5.3 %fusion.85 = f32[2,16,1,64,128]{4,3,2,1,0:T(8,128)S(1)} fusion(f32[4,2,16,1,64,128]{5,4,2,1,3,0:T(8,128)} %bitcast.639, f32[8,16,1,64,128]{4,3,2,1,0:T(8,128)} %all-gather.16.cloned.1.call-done, f32[8,16,1,64,128]{4,3,1,0,2:T(8,128)} %bitcast.636, f32[2,16,64]{2,1,0:T(8,128)S(1)} %get-tuple-element.197, f32[2,16,64]{2,1,0:T(8,128)S(1)} %get-tuple-element.205, ...), kind=kLoop, calls=%fused_computation.124 | loop fusion | flops 6291456 | bytes 9510920 | tf_op jit(solution)/shard_map/add | solution.py:59
  179.3 43.5 %all-gather.10.cloned.1.call-done = f32[4,2,16,1,64,128]{5,4,3,2,1,0:T(8,128)} async-done(((f32[1,2,16,1,64,128]{5,4,3,2,1,0:T(8,128)}), f32[4,2,16,1,64,128]{5,4,3,2,1,0:T(8,128)}) %all-gather.10.cloned.1.call-update) | async-done | bytes 4194320 | tf_op jit(solution)/shard_map/all_gather | solution.py:24
  222.8 5.3 %fusion.92 = f32[2,16,1,64,128]{4,3,2,1,0:T(8,128)S(1)} fusion(f32[4,2,16,1,64,128]{5,4,2,1,3,0:T(8,128)} %bitcast.640, f32[8,16,1,64,128]{4,3,1,0,2:T(8,128)} %bitcast.638, f32[8,16,1,64,128]{4,3,2,1,0:T(8,128)} %all-gather.14.cloned.1.call-done, f32[2,16,64]{2,1,0:T(8,128)S(1)} %get-tuple-element.207, f32[2,16,64]{2,1,0:T(8,128)S(1)} %get-tuple-element.214, ...), kind=kLoop, calls=%fused_computation.135 | loop fusion | flops 6291456 | bytes 9510920 | tf_op jit(solution)/shard_map/add | solution.py:59
  229.3 179.2 %while.18 = (s32[]{:T(128)}, bf16[16,1,64,64]{3,2,1,0:T(8,128)(2,1)}, bf16[16,1,64,64]{3,2,1,0:T(8,128)(2,1)}, bf16[16,1,64,128]{3,2,1,0:T(8,128)(2,1)}, f32[16,...) while((s32[]{:T(128)}, ...), condition=%wide.region_5.6_spmd, body=%wide.region_2.5_spmd.sunk | while | flops 45867008 | bytes 2302909 | solution.py:180
  235.2 1.5 bitcast_dynamic-update-slice_fusion.6
  238.3 1.5 fusion.231
  246.4 1.5 bitcast_dynamic-update-slice_fusion.6
  249.5 1.5 fusion.231
  257.6 1.5 bitcast_dynamic-update-slice_fusion.6
  260.7 1.5 fusion.231
  268.8 1.5 bitcast_dynamic-update-slice_fusion.6
  271.9 1.5 fusion.231
  280.0 1.5 bitcast_dynamic-update-slice_fusion.6
  283.1 1.5 fusion.231
  291.2 1.5 bitcast_dynamic-update-slice_fusion.6
  294.3 1.5 fusion.231
  302.4 1.5 bitcast_dynamic-update-slice_fusion.6
  305.5 1.5 fusion.231
  313.6 1.5 bitcast_dynamic-update-slice_fusion.6
  316.7 1.5 fusion.231
  324.8 1.5 bitcast_dynamic-update-slice_fusion.6
  327.9 1.5 fusion.231
  336.0 1.5 bitcast_dynamic-update-slice_fusion.6
  339.1 1.5 fusion.231
  347.2 1.5 bitcast_dynamic-update-slice_fusion.6
  350.3 1.5 fusion.231
  358.4 1.5 bitcast_dynamic-update-slice_fusion.6
  361.5 1.5 fusion.231
  369.6 1.5 bitcast_dynamic-update-slice_fusion.6
  372.7 1.5 fusion.231
  380.8 1.5 bitcast_dynamic-update-slice_fusion.6
  383.9 1.5 fusion.231
  392.0 1.5 bitcast_dynamic-update-slice_fusion.6
  395.1 1.5 fusion.231
  403.2 1.5 bitcast_dynamic-update-slice_fusion.6
  406.3 1.5 fusion.231
  408.5 2.2 convolution_bitcast_fusion
  410.9 3.1 convolution_convert_fusion
  414.0 6.2 %copy.121 = bf16[16,64,1024]{1,0,2:T(8,128)(2,1)} copy(bf16[16,64,1024]{2,1,0:T(8,128)(2,1)} %convolution_convert_fusion) | data formatting | bytes 4194304
  420.2 6.6 %reshape.1180 = bf16[1024,1024]{1,0:T(8,128)(2,1)} reshape(bf16[1024,16,64]{2,1,0:T(8,128)(2,1)} %bitcast.634) | data formatting | bytes 4194304
  427.0 12.2 %all-gather.4 = f32[8,16,1,64]{3,1,2,0:T(8,128)S(1)} all-gather(f32[2,16,1,64]{3,1,2,0:T(8,128)S(1)} %pad_maximum_fusion.2), channel_id=6, replica_groups=mesh['sp_0'=4,'sp_1'=4,'tp'=8] {'sp_1'}, dimensions={0}, use_global_device_ids=true | all-gather | bytes 40960 | tf_op jit(solution)/shard_map/all_gather | solution.py:24
  439.2 11.9 %all_gather.64 = f32[4,2,16,1,64]{4,2,3,1,0:T(8,128)S(1)} all-gather(f32[1,2,16,1,64]{4,2,3,1,0:T(8,128)S(1)} %fusion.128), channel_id=1, replica_groups=mesh['sp_0'=4,'sp_1'=4,'tp'=8] {'sp_0'}, dimensions={0}, use_global_device_ids=true | all-gather | bytes 40960 | tf_op jit(solution)/shard_map/all_gather | solution.py:24
  451.1 1.7 copy.123
  455.4 13.2 %reduce-scatter.10.cloned.1.call-done = bf16[128,1024]{1,0:T(8,128)(2,1)} async-done(((bf16[1024,1024]{1,0:T(8,128)(2,1)}), bf16[128,1024]{1,0:T(8,128)(2,1)}) %reduce-scatter.10.cloned.1.call-update) | async-done | bytes 262160
  468.6 1.3 reshape.1181
  469.9 1.1 copy.122
  471.0 20.0 %reduce-scatter.12.cloned.1.call-done = f32[64,128]{1,0:T(8,128)} async-done(((f32[256,128]{1,0:T(8,128)}), f32[64,128]{1,0:T(8,128)}) %reduce-scatter.12.cloned.1.call-update) | async-done | bytes 32784
  (529 shorter events, 140.0 us)
Async XLA Ops:
  7.2 3.0 copy-start
  7.2 64.7 %all-gather.16.cloned.1.call-start = ((), (), s32[]{:S(2)}) async-start(), calls=%async_computation.7 | async-start | bytes 5242880 | tf_op jit(solution)/shard_map/all_gather | solution.py:24
  10.1 1.9 copy-start.4
  12.0 7.1 %copy-start.3 = (bf16[16,64,128]{2,1,0:T(8,128)(2,1)S(1)}, bf16[16,64,128]{2,1,0:T(8,128)(2,1)}, u32[]{:S(2)}) copy-start(bf16[16,64,128]{2,1,0:T(8,128)(2,1)} %param.15) | copy-start | bytes 786436
  12.9 5.1 %copy-start.6 = (f32[16,1,64,128]{3,2,0,1:T(8,128)S(1)}, f32[16,1,64,128]{3,2,0,1:T(8,128)}, u32[]{:S(2)}) copy-start(f32[16,1,64,128]{3,2,0,1:T(8,128)} %rev.42) | copy-start | bytes 1572868
  14.3 2.8 copy-start.1
  14.4 3.7 copy-start.2
  18.1 5.6 %copy-start.5 = (f32[16,64,64]{2,0,1:T(8,128)S(1)}, f32[16,64,64]{2,0,1:T(8,128)}, u32[]{:S(2)}) copy-start(f32[16,64,64]{2,0,1:T(8,128)} %get-tuple-element.189) | copy-start | bytes 786436
  21.0 101.0 %all-gather.14.cloned.1.call-start = ((), (), s32[]{:S(2)}) async-start(), calls=%async_computation.6 | async-start | bytes 5242880 | tf_op jit(solution)/shard_map/all_gather | solution.py:24
  26.9 146.0 %all-gather.12.cloned.1.call-start = ((), (), s32[]{:S(2)}) async-start(), calls=%async_computation.4 | async-start | bytes 5242880 | tf_op jit(solution)/shard_map/all_gather | solution.py:24
  75.5 147.4 %all-gather.10.cloned.1.call-start = ((), (), s32[]{:S(2)}) async-start(), calls=%async_computation.3 | async-start | bytes 5242880 | tf_op jit(solution)/shard_map/all_gather | solution.py:24
  125.6 325.5 %reduce-scatter.8.cloned.1.call-start = ((), (), s32[]{:S(2)}) async-start(), calls=%async_computation.5 | async-start | bytes 655360 | tf_op jit(solution)/shard_map/reduce_scatter | solution.py:36
  410.7 57.9 %reduce-scatter.10.cloned.1.call-start = ((), (), s32[]{:S(2)}) async-start(), calls=%async_computation.8 | async-start | bytes 2359296
  420.2 6.7 %copy-start.7 = (f32[16,1,64,64]{3,2,1,0:T(8,128)S(1)}, f32[16,1,64,64]{3,2,1,0:T(8,128)}, u32[]{:S(2)}) copy-start(f32[16,1,64,64]{3,2,1,0:T(8,128)} %get-tuple-element.95) | copy-start | bytes 786436
  426.8 64.2 %reduce-scatter.12.cloned.1.call-start = ((), (), s32[]{:S(2)}) async-start(), calls=%async_computation.9 | async-start | bytes 163840
Sparse Core Ops, SparseCore 0:
  21.1 50.7 all-gather.15
  73.5 48.4 all-gather.13
  123.7 49.1 all-gather.11
  174.4 48.3 all-gather.9
  410.8 22.0 reduce-scatter.7
  435.2 33.3 reduce-scatter.9
  471.5 19.5 reduce-scatter.11
where the time goes:
time: 507 us; the launch traced here: 498 us
  waiting for transfers between devices  166 us (33%)
  matrix products  146 us (29%)
  blocking collectives  73.1 us (14%)
  local copies, waits for them, and re-layouts  66 us (13%)
  other arithmetic  30.7 us (6%)
  between operations  14.5 us (3%)
    all_gather x4, waiting for transfers between devices, prefix_by_axis(): pieces = jax.tree.map(lambda part: lax.all_gather(part, axis), running)  133 us
    all_gather x6, blocking collectives, prefix_by_axis(): pieces = jax.tree.map(lambda part: lax.all_gather(part, axis), running)  73.1 us
    dot_general x32, matrix products, block_grads(): jnp.einsum('hde,hje->hjd', grad_in, value_real, precision=EXACT_DOTS)  39.8 us
    dot_general x32, matrix products, block_grads(): jnp.einsum('hjd,hde->hje', key_seq * to_end, grad_in, precision=EXACT_DOTS)  39.7 us
    unnamed x9, waiting for transfers between devices  33.3 us
    dot_general x32, matrix products, block_grads(): jnp.einsum('hce,hde->hcd', seed_real, state_in, precision=EXACT_DOTS)  29.7 us
    unnamed x23, local copies, waits for them, and re-layouts  18.9 us
    add x4, other arithmetic, compose(): return (earlier[0] * later[0], later[0][..., None] * earlier[1] + later[1])  17.8 us
  transfers between devices with their start and end apart: 7, of which 6 were waited for; matrix products, arithmetic and copies ran while one was open for 8% of the time, Pallas kernels for 0%

commit v1 on v0

v1 whole, which is shorter than its diff:
```python
import functools

import jax
import jax.numpy as jnp
from jax import lax
from jax.experimental import pallas as pl
from jax.experimental.pallas import tpu as pltpu
from jax.sharding import PartitionSpec as P

MESH = pl.DeviceIdType.MESH
F32, BF16 = jnp.float32, jnp.bfloat16
SP, TP = 16, 8
BATCH, TOK, DK, DV, WIDTH = 16, 64, 64, 128, 1024
ROWS = BATCH * TOK
BLK = 256
NBLK = ROWS // BLK
STEP = 2.0**-16
QK, DEC, DO, VV, DVT, DQK, GG, GW = range(8)


def iota(shape, axis):
    return lax.broadcasted_iota(jnp.int32, shape, axis)


def dot(a, b):
    return lax.dot_general(a, b, (((1,), (0,)), ((), ())), preferred_element_type=F32)


def dot_nt(a, b):
    return lax.dot_general(a, b, (((1,), (1,)), ((), ())), preferred_element_type=F32)


def dot_tn(a, b):
    return lax.dot_general(a, b, (((0,), (0,)), ((), ())), preferred_element_type=F32)


def hi_lo(x):
    hi = x.astype(BF16)
    lo = (x - hi.astype(F32)).astype(BF16)
    return jnp.concatenate([hi, lo], axis=1)


def tri(group):
    r, c = iota((BLK, BLK), 0), iota((BLK, BLK), 1)
    keep = r >= c
    if group < BLK:
        keep = keep & (r // group == c // group)
    return jnp.where(keep, 1.0, 0.0).astype(BF16)


def tile(ref, index):
    return ref.at[pl.ds(pl.multiple_of(index * TOK, TOK), TOK)]


def kernel(
    hidden,
    weight,
    q_hbm,
    k_hbm,
    df_hbm,
    db_hbm,
    cot,
    dq_out,
    dk_out,
    gf_out,
    gb_out,
    gh_out,
    gw_out,
    hid,
    w,
    q_in,
    k_in,
    df_in,
    db_in,
    sends,
    recvs,
    qhat,
    khat,
    grow,
    gsum,
    gcum,
    parts,
    dall,
    wx,
    acc,
    hid_t,
    in_sem,
    ss,
    rs,
    loc_sem,
    wss,
    wrs,
    xss,
    xrs,
    pss,
    prs,
):
    me = lax.axis_index("sp")
    tp = lax.axis_index("tp")
    y, z = me % 4, me // 4
    core, xc = tp % 2, tp // 2

    loads = [
        pltpu.make_async_copy(q_hbm, q_in, in_sem.at[0]),
        pltpu.make_async_copy(k_hbm, k_in, in_sem.at[1]),
        pltpu.make_async_copy(df_hbm, df_in, in_sem.at[2]),
        pltpu.make_async_copy(db_hbm, db_in, in_sem.at[3]),
        pltpu.make_async_copy(cot, sends.at[DO], in_sem.at[4]),
        pltpu.make_async_copy(weight, w, in_sem.at[5]),
        pltpu.make_async_copy(hidden, hid, in_sem.at[6]),
    ]
    for load in loads:
        load.start()

    barrier = pltpu.get_barrier_semaphore()

    def greet_sp(r, carry):
        pl.semaphore_signal(
            barrier, inc=1, device_id={"sp": (me + r) % SP}, device_id_type=MESH
        )
        return carry

    def greet_tp(r, carry):
        pl.semaphore_signal(
            barrier, inc=1, device_id={"tp": (tp + r) % TP}, device_id_type=MESH
        )
        return carry

    lax.fori_loop(1, SP, greet_sp, 0)
    lax.fori_loop(1, TP, greet_tp, 0)

    def peer_of(r):
        m = (r * 7) % SP
        return ((z + m // 4) % 4) * 4 + (y + m % 4) % 4

    def sp_copy(kind, r):
        to = peer_of(r)
        src = tile(sends.at[kind], to)
        if kind == DVT:
            dst = dall.at[pl.ds(pl.multiple_of(tp * ROWS + me * TOK, TOK), TOK)]
        else:
            dst = tile(recvs.at[kind], me)
        return pltpu.make_async_remote_copy(
            src_ref=src,
            dst_ref=dst,
            send_sem=ss.at[kind, r],
            recv_sem=rs.at[kind, me],
            device_id={"sp": to},
            device_id_type=MESH,
        )

    def sp_arrived(kind, r):
        frm = peer_of(r)
        if kind == DVT:
            dst = dall.at[pl.ds(pl.multiple_of(tp * ROWS + frm * TOK, TOK), TOK)]
        else:
            dst = tile(recvs.at[kind], frm)
        pltpu.make_async_remote_copy(
            src_ref=dst,
            dst_ref=dst,
            send_sem=ss.at[kind, r],
            recv_sem=rs.at[kind, frm],
            device_id={"sp": frm},
            device_id_type=MESH,
        ).wait_recv()

    def own_copy(kind):
        if kind == DVT:
            dst = dall.at[pl.ds(pl.multiple_of(tp * ROWS + me * TOK, TOK), TOK)]
        else:
            dst = tile(recvs.at[kind], me)
        return pltpu.make_async_copy(tile(sends.at[kind], me), dst, loc_sem.at[kind])

    def send_all(kind):
        def body(r, carry):
            sp_copy(kind, r).start()
            return carry

        lax.fori_loop(1, SP, body, 0)
        own_copy(kind).start()

    def wait_all(kind):
        def body(r, carry):
            sp_arrived(kind, r)
            return carry

        lax.fori_loop(1, SP, body, 0)
        own_copy(kind).wait()

    loads[0].wait()
    loads[1].wait()
    sends[QK] = jnp.concatenate(
        [q_in[...].reshape(ROWS, DK), k_in[...].reshape(ROWS, DK)], axis=1
    )
    loads[2].wait()
    loads[3].wait()
    low = tri(TOK)
    for b in range(NBLK):
        span = pl.ds(b * 4, 4)
        both = jnp.concatenate(
            [df_in[span].reshape(BLK, DK), db_in[span].reshape(BLK, DK)], axis=1
        )
        run = dot(low, hi_lo(both))
        steps = jnp.round((run[:, :DV] + run[:, DV:]) * (1.0 / STEP))
        before = jnp.where(iota((BLK, DV), 0) % TOK == 0, 0.0, pltpu.roll(steps, 1, 0))
        sends[DEC, pl.ds(b * BLK, BLK)] = ((steps - before) * STEP).astype(BF16)
    loads[4].wait()
    loads[5].wait()
    pl.semaphore_wait(barrier, SP + TP - 2)
    send_all(DEC)
    send_all(QK)
    send_all(DO)

    def w_copy(r):
        to = (tp + r) % TP
        return pltpu.make_async_remote_copy(
            src_ref=w.at[pl.ds(pl.multiple_of(to * DV, DV), DV)],
            dst_ref=wx.at[pl.ds(pl.multiple_of(tp * DV, DV), DV)],
            send_sem=wss.at[r],
            recv_sem=wrs.at[r],
            device_id={"tp": to},
            device_id_type=MESH,
        )

    def w_send(r, carry):
        w_copy(r).start()
        return carry

    lax.fori_loop(1, TP, w_send, 0)
    own_w = pltpu.make_async_copy(
        w.at[pl.ds(pl.multiple_of(tp * DV, DV), DV)],
        wx.at[pl.ds(pl.multiple_of(tp * DV, DV), DV)],
        wrs.at[0],
    )
    own_w.start()

    loads[6].wait()
    for b in range(NBLK):
        rows = hid[pl.ds(b * 4, 4)].reshape(BLK, WIDTH)
        sends[VV, pl.ds(b * BLK, BLK)] = dot(rows, w[...]).astype(BF16)
    send_all(VV)

    def turn(t, carry):
        at = pl.ds(pl.multiple_of(t * 128, 128), 128)
        hid_t[:, at] = hid[pl.ds(t * 2, 2)].reshape(128, WIDTH).T
        return carry

    lax.fori_loop(0, ROWS // 128, turn, 0)

    wait_all(DEC)
    lane_f = iota((BLK, DV), 1) < DK
    full = tri(BLK)
    base = jnp.zeros((1, DV), F32)
    cums = []
    for b in range(NBLK):
        d = recvs[DEC, pl.ds(b * BLK, BLK)]
        inside = dot(full, d) + base
        base = inside[BLK - 1 :, :]
        cums.append(jnp.where(lane_f, inside, d.astype(F32) - inside))
    wait_all(QK)
    for b in range(NBLK):
        at = pl.ds(b * BLK, BLK)
        growth = jnp.exp(cums[b])
        shrink = jnp.exp(-cums[b])
        qk = recvs[QK, at].astype(F32)
        kq = pltpu.roll(qk, DK, 1)
        qhat[at] = (jnp.where(lane_f, qk, kq) * growth).astype(BF16)
        khat[at] = (jnp.where(lane_f, kq, qk) * shrink).astype(BF16)
        grow[at] = growth
    wait_all(DO)
    row_f = iota((DV, DV), 0) < DK

    def others(pieces):
        result = []
        zero = jnp.zeros((DV, DV), F32)
        after = [zero] * NBLK
        before = [zero] * NBLK
        for b in range(NBLK - 2, -1, -1):
            after[b] = after[b + 1] + pieces[b + 1]
        for b in range(1, NBLK):
            before[b] = before[b - 1] + pieces[b - 1]
        return after, before

    pieces = [
        dot_tn(qhat[pl.ds(b * BLK, BLK)], recvs[DO, pl.ds(b * BLK, BLK)]) for b in range(NBLK)
    ]
    after, before = others(pieces)
    for b in range(NBLK):
        parts[0, pl.ds(b * DV, DV)] = jnp.where(row_f, after[b], before[b]).astype(BF16)

    r_, c_ = iota((BLK, BLK), 0), iota((BLK, BLK), 1)
    zero16 = jnp.zeros((), BF16)
    for jj in range(NBLK):
        blk = (z + jj) % NBLK
        at = pl.ds(pl.multiple_of(blk * BLK, BLK), BLK)
        pat = pl.ds(pl.multiple_of(blk * DV, DV), DV)
        qh, kh, do = qhat[at], khat[at], recvs[DO, at]
        fwd = dot_nt(jnp.where(lane_f, kh, zero16), qh)
        bwd = dot_nt(jnp.where(lane_f, zero16, kh), qh)
        scores = jnp.where(r_ <= c_, fwd, 0.0) + jnp.where(r_ >= c_, bwd, 0.0)
        dv = dot(kh, parts[0, pat]) + dot(scores.astype(BF16), do)
        sends[DVT, at] = dv.astype(BF16)
        for i in range(4):
            a = (y + i) % 4

            def go(a=a, jj=jj, blk=blk):
                to = blk * 4 + a
                pltpu.make_async_remote_copy(
                    src_ref=tile(sends.at[DVT], to),
                    dst_ref=dall.at[pl.ds(pl.multiple_of(tp * ROWS + me * TOK, TOK), TOK)],
                    send_sem=ss.at[DVT, jj * 4 + i],
                    recv_sem=rs.at[DVT, me],
                    device_id={"sp": to},
                    device_id_type=MESH,
                ).start()

            if jj == 0 and i == 0:
                own_copy(DVT).start()
            else:
                go()

    wait_all(VV)
    pieces = [
        dot_tn(khat[pl.ds(b * BLK, BLK)], recvs[VV, pl.ds(b * BLK, BLK)]) for b in range(NBLK)
    ]
    after, before = others(pieces)
    for b in range(NBLK):
        parts[1, pl.ds(b * DV, DV)] = jnp.where(row_f, before[b], after[b]).astype(BF16)
    base = jnp.zeros((1, DV), F32)
    for b in range(NBLK):
        at = pl.ds(b * BLK, BLK)
        pat = pl.ds(b * DV, DV)
        qh, kh, do, v = qhat[at], khat[at], recvs[DO, at], recvs[VV, at]
        growth = grow[at]
        s = dot_nt(do, v).astype(BF16)
        st = dot_nt(v, do).astype(BF16)
        x = dot_nt(do, parts[1, pat])
        x = x + dot(jnp.where(r_ >= c_, s, zero16), jnp.where(lane_f, kh, zero16))
        x = x + dot(jnp.where(r_ <= c_, s, zero16), jnp.where(lane_f, zero16, kh))
        yk = dot_nt(v, parts[0, pat])
        yk = yk + dot(jnp.where(r_ <= c_, st, zero16), jnp.where(lane_f, qh, zero16))
        yk = yk + dot(jnp.where(r_ >= c_, st, zero16), jnp.where(lane_f, zero16, qh))
        g = qh.astype(F32) * x - kh.astype(F32) * yk
        run = dot(full, hi_lo(g))
        run = run[:, :DV] + run[:, DV:] + base
        base = run[BLK - 1 :, :]
        sends[GG, at] = jnp.where(lane_f, g - run, run).astype(BF16)
        dq2 = x * growth
        dk2 = yk / growth
        dq2 = dq2 + pltpu.roll(dq2, DK, 1)
        dk2 = dk2 + pltpu.roll(dk2, DK, 1)
        sends[DQK, at] = jnp.where(lane_f, dq2, dk2).astype(BF16)
    send_all(DQK)
    send_all(GG)

    wait_all(DVT)
    chip = ((xc + 1) % 4, (xc + 3) % 4, (xc + 2) % 4)

    def head(index):
        return dall.at[pl.ds(pl.multiple_of(index * ROWS, ROWS), ROWS)]

    def x_copy(i):
        return pltpu.make_async_remote_copy(
            src_ref=head(tp),
            dst_ref=head(tp),
            send_sem=xss.at[i],
            recv_sem=xrs.at[i],
            device_id={"tp": chip[i] * 2 + core},
            device_id_type=MESH,
        )

    def x_arrived(i):
        frm = (chip[1], chip[0], chip[2])[i]
        spot = head(frm * 2 + core)
        pltpu.make_async_remote_copy(
            src_ref=spot,
            dst_ref=spot,
            send_sem=xss.at[i],
            recv_sem=xrs.at[i],
            device_id={"tp": frm * 2 + core},
            device_id_type=MESH,
        ).wait_recv()
        return frm

    def p_copy(i, index):
        return pltpu.make_async_remote_copy(
            src_ref=head(index),
            dst_ref=head(index),
            send_sem=pss.at[i],
            recv_sem=prs.at[i],
            device_id={"tp": xc * 2 + 1 - core},
            device_id_type=MESH,
        )

    for i in range(3):
        x_copy(i).start()
    p_copy(3, tp).start()
    drows = dall[pl.ds(pl.multiple_of(tp * ROWS, ROWS), ROWS)]
    for b in range(NBLK):
        at = pl.ds(b * BLK, BLK)
        sends[GW, at] = dot(hid_t[at], drows).astype(BF16)
    send_all(GW)

    wait_all(DQK)
    for b in range(NBLK):
        at = pl.ds(b * BLK, BLK)
        both = recvs[DQK, at]
        dq_out[pl.ds(b * 4, 4)] = both[:, :DK].reshape(4, TOK, DK)
        dk_out[pl.ds(b * 4, 4)] = both[:, DK:].reshape(4, TOK, DK)
    wait_all(GG)
    for b in range(NBLK):
        at = pl.ds(b * BLK, BLK)
        both = recvs[GG, at].astype(F32)
        gf_out[pl.ds(b * 4, 4)] = both[:, :DK].reshape(4, TOK, DK)
        gb_out[pl.ds(b * 4, 4)] = both[:, DK:].reshape(4, TOK, DK)

    def w_arrived(r, carry):
        frm = (tp + TP - r) % TP
        spot = wx.at[pl.ds(pl.multiple_of(frm * DV, DV), DV)]
        pltpu.make_async_remote_copy(
            src_ref=spot,
            dst_ref=spot,
            send_sem=wss.at[r],
            recv_sem=wrs.at[r],
            device_id={"tp": frm},
            device_id_type=MESH,
        ).wait_recv()
        return carry

    lax.fori_loop(1, TP, w_arrived, 0)
    own_w.wait()

    def term(index):
        rows = dall[pl.ds(pl.multiple_of(index * ROWS, ROWS), ROWS)]
        return dot_nt(rows, wx[pl.ds(pl.multiple_of(index * DV, DV), DV)])

    other = xc * 2 + 1 - core
    p_copy(3, other).wait_recv()
    acc[...] = term(tp) + term(other)
    for i in range(3):
        frm = x_arrived(i)
        p_copy(i, frm * 2 + core).start()
        acc[...] += term(frm * 2 + core)
        p_copy(i, frm * 2 + 1 - core).wait_recv()
        if i < 2:
            acc[...] += term(frm * 2 + 1 - core)
        else:
            gh_out[...] = (acc[...] + term(frm * 2 + 1 - core)).astype(BF16).reshape(BATCH, TOK, DV)

    wait_all(GW)
    total = jnp.zeros((TOK, DV), F32)
    for b in range(SP):
        total = total + recvs[GW, pl.ds(b * TOK, TOK)].astype(F32)
    gw_out[...] = total

    def left(r, carry):
        for kind in range(8):
            sp_copy(kind, r).wait_send()
        return carry

    lax.fori_loop(1, SP, left, 0)

    def w_left(r, carry):
        w_copy(r).wait_send()
        return carry

    lax.fori_loop(1, TP, w_left, 0)
    for i in range(3):
        x_copy(i).wait_send()
        p_copy(i, tp).wait_send()
    p_copy(3, tp).wait_send()


def per_device(hidden, value_weight, queries, key_vectors, forward_decay, backward_decay, cotangent):
    any_space = pl.BlockSpec(memory_space=pl.ANY)
    vmem = pl.BlockSpec(memory_space=pltpu.VMEM)
    narrow = (BATCH, TOK, DK)
    sem = pltpu.SemaphoreType.DMA
    outs = pl.pallas_call(
        kernel,
        out_shape=(
            jax.ShapeDtypeStruct(narrow, BF16),
            jax.ShapeDtypeStruct(narrow, BF16),
            jax.ShapeDtypeStruct(narrow, F32),
            jax.ShapeDtypeStruct(narrow, F32),
            jax.ShapeDtypeStruct((BATCH, TOK, DV), BF16),
            jax.ShapeDtypeStruct((WIDTH // SP, DV), F32),
        ),
        in_specs=[any_space] * 7,
        out_specs=(vmem,) * 6,
        scratch_shapes=[
            pltpu.VMEM((BATCH, TOK, WIDTH), BF16),
            pltpu.VMEM((WIDTH, DV), BF16),
            pltpu.VMEM(narrow, BF16),
            pltpu.VMEM(narrow, BF16),
            pltpu.VMEM(narrow, F32),
            pltpu.VMEM(narrow, F32),
            pltpu.VMEM((8, ROWS, DV), BF16),
            pltpu.VMEM((8, ROWS, DV), BF16),
            pltpu.VMEM((ROWS, DV), BF16),
            pltpu.VMEM((ROWS, DV), BF16),
            pltpu.VMEM((ROWS, DV), F32),
            pltpu.VMEM((8, DV), F32),
            pltpu.VMEM((8, DV), F32),
            pltpu.VMEM((2, NBLK * DV, DV), BF16),
            pltpu.VMEM((TP * ROWS, DV), BF16),
            pltpu.VMEM((TP * DV, DV), BF16),
            pltpu.VMEM((ROWS, DV), F32),
            pltpu.VMEM((WIDTH, ROWS), BF16),
            sem((7,)),
            sem((8, SP)),
            sem((8, SP)),
            sem((8,)),
            sem((TP,)),
            sem((TP,)),
            sem((3,)),
            sem((3,)),
            sem((4,)),
            sem((4,)),
        ],
        compiler_params=pltpu.CompilerParams(
            collective_id=0, has_side_effects=True, vmem_limit_bytes=60 << 20
        ),
    )(
        hidden,
        value_weight,
        queries.reshape(narrow),
        key_vectors.reshape(narrow),
        forward_decay.reshape(narrow),
        backward_decay.reshape(narrow),
        cotangent.reshape(ROWS, DV),
    )
    heads = (BATCH, 1, TOK, DK)
    return tuple(out.reshape(heads) for out in outs[:4]) + tuple(outs[4:])


def solution(mesh):
    spread = P(None, "tp", "sp", None)
    return jax.shard_map(
        per_device,
        mesh=mesh,
        in_specs=(
            P(None, "sp", None),
            P(None, "tp"),
            spread,
            spread,
            spread,
            spread,
            P(None, "sp", "tp"),
        ),
        out_specs=(spread, spread, spread, spread, P(None, "sp", "tp"), P("sp", "tp")),
        check_vma=False,
    )
```

time: 507 us -> 57.1 us (0.11)
  the two profiles are of different devices: /device:TPU:0 before, /device:TPU:1 now
where the time goes in v1:
time: 57.1 us; the launch traced here: 56.9 us
  Pallas kernels  48.9 us (86%)
  local copies, waits for them, and re-layouts  7.42 us (13%)
  between operations  0.67 us (1%)
    pallas_call x1, Pallas kernels, per_device(): pl.pallas_call(kernel, out_shape=(jax.ShapeDtypeStruct(narrow, BF16), jax...  48.9 us
    unnamed x12, local copies, waits for them, and re-layouts  7.42 us

profile of v1, /device:TPU:1, one launch (start us, length us, event | category | flops | bytes accessed | tf_op | source)
XLA Modules:
  0.0 56.9 jit_solution(6617959665681556199)
XLA Ops:
  0.6 48.9 %shard_map.118 = (bf16[16,64,64]{2,1,0:T(8,128)(2,1)}, bf16[16,64,64]{2,1,0:T(8,128)(2,1)}, f32[16,64,64]{2,1,0:T(8,128)}, f32[16,64,64]{2,1,0:T(8,128)}, bf16[1...) custom-call(bf16[16,64,1024]{2,1,0:T(8,128)(2,1)} %hidden.1, bf16[1024,128]{1,0:T(8,128)(2,1)} %weight.1, ...), custom_call_target="tpu_custom_call" | custom-call | tf_op jit(solution)/shard_map/pallas_call | solution.py:479
  49.5 0.0 copy-start
  49.5 0.0 copy-start.1
  49.5 0.0 copy-start.2
  49.5 1.7 %copy.23 = bf16[16,1,64,64]{3,2,1,0:T(8,128)(2,1)} copy(bf16[16,1,64,64]{3,2,1,0:T(8,128)(2,1)} %bitcast.25) | data formatting | bytes 262144
  51.3 1.7 %copy.24 = bf16[16,1,64,64]{3,2,1,0:T(8,128)(2,1)} copy(bf16[16,1,64,64]{3,2,1,0:T(8,128)(2,1)} %bitcast.24) | data formatting | bytes 262144
  52.9 1.9 %copy.25 = f32[16,1,64,64]{3,2,1,0:T(8,128)} copy(f32[16,1,64,64]{3,2,1,0:T(8,128)} %bitcast.18) | data formatting | bytes 524288
  54.8 0.0 copy-done
  54.8 0.8 %copy.26 = f32[16,1,64,64]{3,2,1,0:T(8,128)} copy(f32[16,1,64,64]{3,2,1,0:T(8,128)S(1)} %bitcast.17) | data formatting | bytes 524288
  55.6 0.0 copy-done.1
  55.6 0.7 %copy.27 = bf16[16,64,128]{2,1,0:T(8,128)(2,1)} copy(bf16[16,64,128]{2,1,0:T(8,128)(2,1)S(1)} %copy-done.1) | data formatting | bytes 524288
  56.3 0.0 copy-done.2
  56.3 0.6 %copy.28 = f32[64,128]{1,0:T(8,128)} copy(f32[64,128]{1,0:T(8,128)S(1)} %copy-done.2) | data formatting | bytes 65536
Async XLA Ops:
  49.5 5.3 %copy-start = (f32[16,64,64]{2,1,0:T(8,128)S(1)}, f32[16,64,64]{2,1,0:T(8,128)}, u32[]{:S(2)}) copy-start(f32[16,64,64]{2,1,0:T(8,128)} %get-tuple-element.15) | copy-start | bytes 786436
  49.5 6.1 %copy-start.1 = (bf16[16,64,128]{2,1,0:T(8,128)(2,1)S(1)}, bf16[16,64,128]{2,1,0:T(8,128)(2,1)}, u32[]{:S(2)}) copy-start(bf16[16,64,128]{2,1,0:T(8,128)(2,1)} %get-tuple-element.34) | copy-start | bytes 786436
  49.5 6.8 %copy-start.2 = (f32[64,128]{1,0:T(8,128)S(1)}, f32[64,128]{1,0:T(8,128)}, u32[]{:S(2)}) copy-start(f32[64,128]{1,0:T(8,128)} %get-tuple-element.35) | copy-start | bytes 98308

commit v2 on v1

v2 whole, which is shorter than its diff:
```python
import functools

import jax
import jax.numpy as jnp
from jax import lax
from jax.experimental import pallas as pl
from jax.experimental.pallas import tpu as pltpu
from jax.sharding import PartitionSpec as P

MESH = pl.DeviceIdType.MESH
F32, BF16 = jnp.float32, jnp.bfloat16
SP, TP = 16, 8
BATCH, TOK, DK, DV, WIDTH = 16, 64, 64, 128, 1024
ROWS = BATCH * TOK
BLK = 256
NBLK = ROWS // BLK
STEP = 2.0**-16
QK, DEC, DO, VV, DVT, DQK, GG, GW = range(8)


def iota(shape, axis):
    return lax.broadcasted_iota(jnp.int32, shape, axis)


def dot(a, b):
    return lax.dot_general(a, b, (((1,), (0,)), ((), ())), preferred_element_type=F32)


def dot_nt(a, b):
    return lax.dot_general(a, b, (((1,), (1,)), ((), ())), preferred_element_type=F32)


def dot_tn(a, b):
    return lax.dot_general(a, b, (((0,), (0,)), ((), ())), preferred_element_type=F32)


def hi_lo(x):
    hi = x.astype(BF16)
    lo = (x - hi.astype(F32)).astype(BF16)
    return jnp.concatenate([hi, lo], axis=1)


def tri(group):
    r, c = iota((BLK, BLK), 0), iota((BLK, BLK), 1)
    keep = r >= c
    if group < BLK:
        keep = keep & (r // group == c // group)
    return jnp.where(keep, 1.0, 0.0).astype(BF16)


def tile(ref, index):
    return ref.at[pl.ds(pl.multiple_of(index * TOK, TOK), TOK)]


def kernel(
    hidden,
    weight,
    q_hbm,
    k_hbm,
    df_hbm,
    db_hbm,
    cot,
    dqk_out,
    gg_out,
    gh_out,
    gw_out,
    hid,
    w,
    q_in,
    k_in,
    df_in,
    db_in,
    sends,
    recvs,
    qhat,
    khat,
    grow,
    gterm,
    scores,
    parts,
    dall,
    wx,
    acc,
    hid_t,
    in_sem,
    ss,
    rs,
    loc_sem,
    wss,
    wrs,
    xss,
    xrs,
    pss,
    prs,
):
    me = lax.axis_index("sp")
    tp = lax.axis_index("tp")
    y, z = me % 4, me // 4
    core, xc = tp % 2, tp // 2
    barrier = pltpu.get_barrier_semaphore()

    def greet_sp(r, carry):
        pl.semaphore_signal(
            barrier, inc=1, device_id={"sp": (me + r) % SP}, device_id_type=MESH
        )
        return carry

    def greet_tp(r, carry):
        pl.semaphore_signal(
            barrier, inc=1, device_id={"tp": (tp + r) % TP}, device_id_type=MESH
        )
        return carry

    lax.fori_loop(1, SP, greet_sp, 0)
    lax.fori_loop(1, TP, greet_tp, 0)

    loads = [
        pltpu.make_async_copy(df_hbm, df_in, in_sem.at[2]),
        pltpu.make_async_copy(db_hbm, db_in, in_sem.at[3]),
        pltpu.make_async_copy(q_hbm, q_in, in_sem.at[0]),
        pltpu.make_async_copy(k_hbm, k_in, in_sem.at[1]),
        pltpu.make_async_copy(cot, sends.at[DO], in_sem.at[4]),
        pltpu.make_async_copy(weight, w, in_sem.at[5]),
        pltpu.make_async_copy(hidden, hid, in_sem.at[6]),
    ]
    for load in loads:
        load.start()

    def peer_of(r):
        m = (r * 7) % SP
        return ((z + m // 4) % 4) * 4 + (y + m % 4) % 4

    def landing(kind, frm):
        if kind == DVT:
            return dall.at[pl.ds(pl.multiple_of(tp * ROWS + frm * TOK, TOK), TOK)]
        return tile(recvs.at[kind], frm)

    def sp_copy(kind, r, to):
        return pltpu.make_async_remote_copy(
            src_ref=tile(sends.at[kind], to),
            dst_ref=landing(kind, me),
            send_sem=ss.at[kind, r],
            recv_sem=rs.at[kind, me],
            device_id={"sp": to},
            device_id_type=MESH,
        )

    def sp_wait(kind, r, frm):
        pltpu.make_async_remote_copy(
            src_ref=landing(kind, frm),
            dst_ref=landing(kind, frm),
            send_sem=ss.at[kind, r],
            recv_sem=rs.at[kind, frm],
            device_id={"sp": frm},
            device_id_type=MESH,
        ).wait_recv()

    def own_copy(kind):
        return pltpu.make_async_copy(
            tile(sends.at[kind], me), landing(kind, me), loc_sem.at[kind]
        )

    def send_all(kind):
        def body(r, carry):
            sp_copy(kind, r, peer_of(r)).start()
            return carry

        lax.fori_loop(1, SP, body, 0)
        own_copy(kind).start()

    def wait_all(kind):
        def body(r, carry):
            sp_wait(kind, r, peer_of(r))
            return carry

        lax.fori_loop(1, SP, body, 0)
        own_copy(kind).wait()

    def send_block(kind, jj, blk):
        for i in range(4):
            if jj == 0 and i == 0:
                own_copy(kind).start()
            else:
                sp_copy(kind, jj * 4 + i, blk * 4 + (y + i) % 4).start()

    def wait_plane(kind, jj, plane):
        for i in range(4):
            if jj == 0 and i == 0:
                own_copy(kind).wait()
            else:
                sp_wait(kind, jj * 4 + i, plane * 4 + (y + i) % 4)

    loads[0].wait()
    loads[1].wait()
    low = tri(TOK)
    for b in range(NBLK):
        span = pl.ds(b * 4, 4)
        both = jnp.concatenate(
            [df_in[span].reshape(BLK, DK), db_in[span].reshape(BLK, DK)], axis=1
        )
        run = dot(low, hi_lo(both))
        steps = jnp.round((run[:, :DV] + run[:, DV:]) * (1.0 / STEP))
        before = jnp.where(iota((BLK, DV), 0) % TOK == 0, 0.0, pltpu.roll(steps, 1, 0))
        sends[DEC, pl.ds(b * BLK, BLK)] = ((steps - before) * STEP).astype(BF16)
    loads[2].wait()
    loads[3].wait()
    sends[QK] = jnp.concatenate(
        [q_in[...].reshape(ROWS, DK), k_in[...].reshape(ROWS, DK)], axis=1
    )
    loads[4].wait()
    loads[5].wait()
    pl.semaphore_wait(barrier, SP + TP - 2)
    send_all(DEC)
    send_all(QK)
    send_all(DO)

    def w_copy(r):
        to = (tp + r) % TP
        return pltpu.make_async_remote_copy(
            src_ref=w.at[pl.ds(pl.multiple_of(to * DV, DV), DV)],
            dst_ref=wx.at[pl.ds(pl.multiple_of(tp * DV, DV), DV)],
            send_sem=wss.at[r],
            recv_sem=wrs.at[r],
            device_id={"tp": to},
            device_id_type=MESH,
        )

    def w_send(r, carry):
        w_copy(r).start()
        return carry

    lax.fori_loop(1, TP, w_send, 0)
    own_w = pltpu.make_async_copy(
        w.at[pl.ds(pl.multiple_of(tp * DV, DV), DV)],
        wx.at[pl.ds(pl.multiple_of(tp * DV, DV), DV)],
        wrs.at[0],
    )
    own_w.start()

    loads[6].wait()
    for b in range(NBLK):
        rows = hid[pl.ds(b * 4, 4)].reshape(BLK, WIDTH)
        sends[VV, pl.ds(b * BLK, BLK)] = dot(rows, w[...]).astype(BF16)
    send_all(VV)

    def turn(t, carry):
        at = pl.ds(pl.multiple_of(t * 128, 128), 128)
        hid_t[:, at] = hid[pl.ds(t * 2, 2)].reshape(128, WIDTH).T
        return carry

    lax.fori_loop(0, ROWS // 128, turn, 0)

    wait_all(DEC)
    lane_f = iota((BLK, DV), 1) < DK
    full = tri(BLK)
    base = jnp.zeros((1, DV), F32)
    cums = []
    for b in range(NBLK):
        d = recvs[DEC, pl.ds(b * BLK, BLK)]
        inside = dot(full, d) + base
        base = inside[BLK - 1 :, :]
        cums.append(jnp.where(lane_f, inside, d.astype(F32) - inside))
    wait_all(QK)
    r_, c_ = iota((BLK, BLK), 0), iota((BLK, BLK), 1)
    zero16 = jnp.zeros((), BF16)
    for b in range(NBLK):
        at = pl.ds(b * BLK, BLK)
        growth = jnp.exp(cums[b])
        shrink = jnp.exp(-cums[b])
        qk = recvs[QK, at].astype(F32)
        kq = pltpu.roll(qk, DK, 1)
        qh = (jnp.where(lane_f, qk, kq) * growth).astype(BF16)
        kh = (jnp.where(lane_f, kq, qk) * shrink).astype(BF16)
        qhat[at] = qh
        khat[at] = kh
        grow[at] = growth
        fwd = dot_nt(jnp.where(lane_f, kh, zero16), qh)
        bwd = dot_nt(jnp.where(lane_f, zero16, kh), qh)
        both = jnp.where(r_ <= c_, fwd, 0.0) + jnp.where(r_ >= c_, bwd, 0.0)
        scores[at] = both.astype(BF16)
    row_f = iota((DV, DV), 0) < DK

    def others(pieces):
        zero = jnp.zeros((DV, DV), F32)
        after, before = [zero] * NBLK, [zero] * NBLK
        for b in range(NBLK - 2, -1, -1):
            after[b] = after[b + 1] + pieces[b + 1]
        for b in range(1, NBLK):
            before[b] = before[b - 1] + pieces[b - 1]
        return after, before

    wait_all(DO)
    pieces = [
        dot_tn(qhat[pl.ds(b * BLK, BLK)], recvs[DO, pl.ds(b * BLK, BLK)]) for b in range(NBLK)
    ]
    after, before = others(pieces)
    for b in range(NBLK):
        parts[0, pl.ds(b * DV, DV)] = jnp.where(row_f, after[b], before[b]).astype(BF16)
    for jj in range(NBLK):
        blk = (z + jj) % NBLK
        at = pl.ds(pl.multiple_of(blk * BLK, BLK), BLK)
        pat = pl.ds(pl.multiple_of(blk * DV, DV), DV)
        dv = dot(khat[at], parts[0, pat]) + dot(scores[at], recvs[DO, at])
        sends[DVT, at] = dv.astype(BF16)
        send_block(DVT, jj, blk)

    right, left, far = (xc + 1) % 4, (xc + 3) % 4, (xc + 2) % 4

    def piece(head, cc):
        row = head * ROWS + ((z + 4 - cc) % 4) * BLK
        return dall.at[pl.ds(pl.multiple_of(row, BLK), BLK)]

    def hop(head, cc, sems_s, sems_r, slot, to):
        return pltpu.make_async_remote_copy(
            src_ref=piece(head, cc),
            dst_ref=piece(head, cc),
            send_sem=sems_s.at[slot, cc],
            recv_sem=sems_r.at[slot, cc],
            device_id={"tp": to},
            device_id_type=MESH,
        )

    def to_chip(head, cc, slot, chip):
        return hop(head, cc, xss, xrs, slot, chip * 2 + core)

    def to_core(head, cc, slot):
        return hop(head, cc, pss, prs, slot, xc * 2 + 1 - core)

    def first_hops(cc):
        wait_plane(DVT, cc, (z + 4 - cc) % 4)
        to_chip(tp, cc, 0, right).start()
        to_chip(tp, cc, 1, left).start()
        to_core(tp, cc, 0).start()

    wait_all(VV)
    pieces = [
        dot_tn(khat[pl.ds(b * BLK, BLK)], recvs[VV, pl.ds(b * BLK, BLK)]) for b in range(NBLK)
    ]
    after, before = others(pieces)
    for b in range(NBLK):
        parts[1, pl.ds(b * DV, DV)] = jnp.where(row_f, before[b], after[b]).astype(BF16)
    for jj in range(NBLK):
        blk = (z + jj) % NBLK
        at = pl.ds(pl.multiple_of(blk * BLK, BLK), BLK)
        pat = pl.ds(pl.multiple_of(blk * DV, DV), DV)
        qh, kh, do, v = qhat[at], khat[at], recvs[DO, at], recvs[VV, at]
        growth = grow[at]
        s = dot_nt(do, v).astype(BF16)
        st = dot_nt(v, do).astype(BF16)
        x = dot_nt(do, parts[1, pat])
        x = x + dot(jnp.where(r_ >= c_, s, zero16), jnp.where(lane_f, kh, zero16))
        x = x + dot(jnp.where(r_ <= c_, s, zero16), jnp.where(lane_f, zero16, kh))
        yk = dot_nt(v, parts[0, pat])
        yk = yk + dot(jnp.where(r_ <= c_, st, zero16), jnp.where(lane_f, qh, zero16))
        yk = yk + dot(jnp.where(r_ >= c_, st, zero16), jnp.where(lane_f, zero16, qh))
        gterm[at] = qh.astype(F32) * x - kh.astype(F32) * yk
        dq2 = x * growth
        dk2 = yk / growth
        dq2 = dq2 + pltpu.roll(dq2, DK, 1)
        dk2 = dk2 + pltpu.roll(dk2, DK, 1)
        sends[DQK, at] = jnp.where(lane_f, dq2, dk2).astype(BF16)
        send_block(DQK, jj, blk)
        first_hops(jj)
    base = jnp.zeros((1, DV), F32)
    for b in range(NBLK):
        at = pl.ds(b * BLK, BLK)
        g = gterm[at]
        run = dot(full, hi_lo(g))
        run = run[:, :DV] + run[:, DV:] + base
        base = run[BLK - 1 :, :]
        sends[GG, at] = jnp.where(lane_f, g - run, run).astype(BF16)

    drows = dall[pl.ds(pl.multiple_of(tp * ROWS, ROWS), ROWS)]
    for b in range(NBLK):
        at = pl.ds(b * BLK, BLK)
        sends[GW, at] = dot(hid_t[at], drows).astype(BF16)
    send_all(GW)
    send_all(GG)

    def w_arrived(r, carry):
        frm = (tp + TP - r) % TP
        spot = wx.at[pl.ds(pl.multiple_of(frm * DV, DV), DV)]
        pltpu.make_async_remote_copy(
            src_ref=spot,
            dst_ref=spot,
            send_sem=wss.at[r],
            recv_sem=wrs.at[r],
            device_id={"tp": frm},
            device_id_type=MESH,
        ).wait_recv()
        return carry

    lax.fori_loop(1, TP, w_arrived, 0)
    own_w.wait()

    def term(chip, cc):
        total = None
        for c in range(2):
            head = chip * 2 + c
            row = head * ROWS + ((z + 4 - cc) % 4) * BLK
            rows = dall[pl.ds(pl.multiple_of(row, BLK), BLK)]
            part = dot_nt(rows, wx[pl.ds(pl.multiple_of(head * DV, DV), DV)])
            total = part if total is None else total + part
        return total

    for cc in range(4):
        head_l, head_r = left * 2 + core, right * 2 + core
        to_chip(head_l, cc, 0, left).wait_recv()
        if cc % 2 == 0:
            to_chip(head_l, cc, 2, right).start()
        to_core(head_l, cc, 1).start()
        to_chip(head_r, cc, 1, right).wait_recv()
        if cc % 2 == 1:
            to_chip(head_r, cc, 2, left).start()
        to_core(head_r, cc, 2).start()
    for cc in range(4):
        for slot, chip in ((0, xc), (1, left), (2, right)):
            to_core(chip * 2 + 1 - core, cc, slot).wait_recv()
        acc[pl.ds(cc * BLK, BLK)] = term(xc, cc) + term(left, cc) + term(right, cc)
    for cc in range(4):
        to_chip(far * 2 + core, cc, 2, far).wait_recv()
        to_core(far * 2 + core, cc, 3).start()

    wait_all(DQK)
    dqk_out[...] = recvs[DQK]
    wait_all(GG)
    gg_out[...] = recvs[GG]
    wait_all(GW)
    total = jnp.zeros((TOK, DV), F32)
    for b in range(SP):
        total = total + recvs[GW, pl.ds(b * TOK, TOK)].astype(F32)
    gw_out[...] = total
    for cc in range(4):
        to_core(far * 2 + 1 - core, cc, 3).wait_recv()
        at = pl.ds(pl.multiple_of(((z + 4 - cc) % 4) * BLK, BLK), BLK)
        gh_out[at] = (acc[pl.ds(cc * BLK, BLK)] + term(far, cc)).astype(BF16)

    def left_here(r, carry):
        for kind in range(8):
            sp_copy(kind, r, peer_of(r)).wait_send()
        return carry

    lax.fori_loop(1, SP, left_here, 0)

    def w_left(r, carry):
        w_copy(r).wait_send()
        return carry

    lax.fori_loop(1, TP, w_left, 0)
    for cc in range(4):
        for slot in range(3):
            to_chip(tp, cc, slot, right).wait_send()
        for slot in range(4):
            to_core(tp, cc, slot).wait_send()


def finish(dqk, gg, gh, gw, dq_out, dk_out, gf_out, gb_out, gh_out, gw_out):
    both = dqk[...]
    dq_out[...] = both[:, :DK].reshape(BATCH, TOK, DK)
    dk_out[...] = both[:, DK:].reshape(BATCH, TOK, DK)
    sums = gg[...].astype(F32)
    gf_out[...] = sums[:, :DK].reshape(BATCH, TOK, DK)
    gb_out[...] = sums[:, DK:].reshape(BATCH, TOK, DK)
    gh_out[...] = gh[...].reshape(BATCH, TOK, DV)
    gw_out[...] = gw[...]


def per_device(hidden, value_weight, queries, key_vectors, forward_decay, backward_decay, cotangent):
    in_hbm = pl.BlockSpec(memory_space=pltpu.HBM)
    vmem = pl.BlockSpec(memory_space=pltpu.VMEM)
    narrow = (BATCH, TOK, DK)
    wide = (ROWS, DV)
    sem = pltpu.SemaphoreType.DMA
    shape = jax.ShapeDtypeStruct
    rows_of = pl.pallas_call(
        kernel,
        out_shape=(shape(wide, BF16), shape(wide, BF16), shape(wide, BF16), shape((WIDTH // SP, DV), F32)),
        in_specs=[in_hbm] * 7,
        out_specs=(vmem,) * 4,
        scratch_shapes=[
            pltpu.VMEM((BATCH, TOK, WIDTH), BF16),
            pltpu.VMEM((WIDTH, DV), BF16),
            pltpu.VMEM(narrow, BF16),
            pltpu.VMEM(narrow, BF16),
            pltpu.VMEM(narrow, F32),
            pltpu.VMEM(narrow, F32),
            pltpu.VMEM((8, ROWS, DV), BF16),
            pltpu.VMEM((8, ROWS, DV), BF16),
            pltpu.VMEM(wide, BF16),
            pltpu.VMEM(wide, BF16),
            pltpu.VMEM(wide, F32),
            pltpu.VMEM(wide, F32),
            pltpu.VMEM((ROWS, BLK), BF16),
            pltpu.VMEM((2, NBLK * DV, DV), BF16),
            pltpu.VMEM((TP * ROWS, DV), BF16),
            pltpu.VMEM((TP * DV, DV), BF16),
            pltpu.VMEM(wide, F32),
            pltpu.VMEM((WIDTH, ROWS), BF16),
            sem((7,)),
            sem((8, SP)),
            sem((8, SP)),
            sem((8,)),
            sem((TP,)),
            sem((TP,)),
            sem((3, 4)),
            sem((3, 4)),
            sem((4, 4)),
            sem((4, 4)),
        ],
        compiler_params=pltpu.CompilerParams(
            collective_id=0, has_side_effects=True, vmem_limit_bytes=26 << 20
        ),
    )(
        *(
            pltpu.with_memory_space_constraint(operand, pltpu.HBM)
            for operand in (
                hidden,
                value_weight,
                queries.reshape(narrow),
                key_vectors.reshape(narrow),
                forward_decay.reshape(narrow),
                backward_decay.reshape(narrow),
                cotangent.reshape(wide),
            )
        )
    )
    outs = pl.pallas_call(
        finish,
        out_shape=(
            shape(narrow, BF16),
            shape(narrow, BF16),
            shape(narrow, F32),
            shape(narrow, F32),
            shape((BATCH, TOK, DV), BF16),
            shape((WIDTH // SP, DV), F32),
        ),
        in_specs=[vmem] * 4,
        out_specs=(vmem,) * 6,
        compiler_params=pltpu.CompilerParams(vmem_limit_bytes=16 << 20),
    )(*rows_of)
    heads = (BATCH, 1, TOK, DK)
    return tuple(out.reshape(heads) for out in outs[:4]) + tuple(outs[4:])


def solution(mesh):
    spread = P(None, "tp", "sp", None)
    return jax.shard_map(
        per_device,
        mesh=mesh,
        in_specs=(
            P(None, "sp", None),
            P(None, "tp"),
            spread,
            spread,
            spread,
            spread,
            P(None, "sp", "tp"),
        ),
        out_specs=(spread, spread, spread, spread, P(None, "sp", "tp"), P("sp", "tp")),
        check_vma=False,
    )
```

time: 57.1 us -> 43.4 us (0.76)
  local copies, waits for them, and re-layouts: 7.42 us -> 0 us
  Pallas kernels: 48.9 us -> 42.6 us
    unnamed x12 -> x0, local copies, waits for them, and re-layouts: 7.42 us -> none
    pallas_call x1 -> x2, Pallas kernels: 48.9 us -> 42.6 us  [the longest x1 41.2 us: per_device(): pl.pallas_call(kernel, out_shape=(shape(wide, BF16), shape(wide, BF16), s...]
where the time goes in v2:
time: 43.4 us; the launch traced here: 43.2 us
  Pallas kernels  42.6 us (98%)
  between operations  0.64 us (1%)
    pallas_call x1, Pallas kernels, per_device(): pl.pallas_call(kernel, out_shape=(shape(wide, BF16), shape(wide, BF16), s...  41.2 us
    pallas_call x1, Pallas kernels, per_device(): pl.pallas_call(finish, out_shape=(shape(narrow, BF16), shape(narrow, BF16...  1.45 us

profile of v2, /device:TPU:1, one launch (start us, length us, event | category | flops | bytes accessed | tf_op | source)
XLA Modules:
  0.0 43.2 jit_solution(224495627339974240)
XLA Ops:
  0.6 41.2 %shard_map.118 = (bf16[1024,128]{1,0:T(8,128)(2,1)S(1)}, bf16[1024,128]{1,0:T(8,128)(2,1)S(1)}, bf16[1024,128]{1,0:T(8,128)(2,1)S(1)}, f32[64,128]{1,0:T(8,128)S(1)}) custom-call(bf16[16,64,1024]{2,1,0:T(8,128)(2,1)} %hidden.1, bf16[1024,128]{1,0:T(8,128)(2,1)} %weight.1, bf16[16,64,64]{2,1,0:T(8,128)(2,1)} %bitcast.19, bf16[16,64,64]{2,1,0:T(8,128)(2,1)} %bitcast.20, ...), custom_call_target="tpu_custom_call" | custom-call | tf_op jit(solution)/shard_map/pallas_call | solution.py:475
  41.8 1.4 %shard_map.119 = (bf16[16,64,64]{2,1,0:T(8,128)(2,1)}, bf16[16,64,64]{2,1,0:T(8,128)(2,1)}, f32[16,64,64]{2,1,0:T(8,128)}, f32[16,64,64]{2,1,0:T(8,128)}, bf16[1...) custom-call(bf16[1024,128]{1,0:T(8,128)(2,1)S(1)} %get-tuple-element.16.dqk, bf16[1024,128]{1,0:T(8,128)(2,1)S(1)} %get-tuple-element.17.gg, ...), custom_call_target="tpu_custom_call" | custom-call | tf_op jit(solution)/shard_map/pallas_call | solution.py:527

commit v3 on v2

--- a/solution.py
+++ b/solution.py
@@ -60,8 +60,10 @@
     df_hbm,
     db_hbm,
     cot,
-    dqk_out,
-    gg_out,
+    dq_out,
+    dk_out,
+    gf_out,
+    gb_out,
     gh_out,
     gw_out,
     hid,
@@ -422,9 +424,15 @@
         to_core(far * 2 + core, cc, 3).start()
 
     wait_all(DQK)
-    dqk_out[...] = recvs[DQK]
+    for b in range(NBLK):
+        both, span = recvs[DQK, pl.ds(b * BLK, BLK)], pl.ds(b * 4, 4)
+        dq_out[span] = both[:, :DK].reshape(4, TOK, DK)
+        dk_out[span] = both[:, DK:].reshape(4, TOK, DK)
     wait_all(GG)
-    gg_out[...] = recvs[GG]
+    for b in range(NBLK):
+        both, span = recvs[GG, pl.ds(b * BLK, BLK)].astype(F32), pl.ds(b * 4, 4)
+        gf_out[span] = both[:, :DK].reshape(4, TOK, DK)
+        gb_out[span] = both[:, DK:].reshape(4, TOK, DK)
     wait_all(GW)
     total = jnp.zeros((TOK, DV), F32)
     for b in range(SP):
@@ -454,15 +462,13 @@
             to_core(tp, cc, slot).wait_send()
 
 
-def finish(dqk, gg, gh, gw, dq_out, dk_out, gf_out, gb_out, gh_out, gw_out):
-    both = dqk[...]
-    dq_out[...] = both[:, :DK].reshape(BATCH, TOK, DK)
-    dk_out[...] = both[:, DK:].reshape(BATCH, TOK, DK)
-    sums = gg[...].astype(F32)
-    gf_out[...] = sums[:, :DK].reshape(BATCH, TOK, DK)
-    gb_out[...] = sums[:, DK:].reshape(BATCH, TOK, DK)
-    gh_out[...] = gh[...].reshape(BATCH, TOK, DV)
-    gw_out[...] = gw[...]
+def finish(*refs):
+    out_sem = refs[-1]
+    copies = [pltpu.make_async_copy(refs[i], refs[i + 6], out_sem.at[i]) for i in (2, 3, 0, 1, 4, 5)]
+    for copy in copies:
+        copy.start()
+    for copy in copies:
+        copy.wait()
 
 
 def per_device(hidden, value_weight, queries, key_vectors, forward_decay, backward_decay, cotangent):
@@ -474,9 +480,16 @@
     shape = jax.ShapeDtypeStruct
     rows_of = pl.pallas_call(
         kernel,
-        out_shape=(shape(wide, BF16), shape(wide, BF16), shape(wide, BF16), shape((WIDTH // SP, DV), F32)),
+        out_shape=(
+            shape(narrow, BF16),
+            shape(narrow, BF16),
+            shape(narrow, F32),
+            shape(narrow, F32),
+            shape(wide, BF16),
+            shape((WIDTH // SP, DV), F32),
+        ),
         in_specs=[in_hbm] * 7,
-        out_specs=(vmem,) * 4,
+        out_specs=(vmem,) * 6,
         scratch_shapes=[
             pltpu.VMEM((BATCH, TOK, WIDTH), BF16),
             pltpu.VMEM((WIDTH, DV), BF16),
@@ -531,15 +544,16 @@
             shape(narrow, BF16),
             shape(narrow, F32),
             shape(narrow, F32),
-            shape((BATCH, TOK, DV), BF16),
+            shape(wide, BF16),
             shape((WIDTH // SP, DV), F32),
         ),
-        in_specs=[vmem] * 4,
-        out_specs=(vmem,) * 6,
+        in_specs=[vmem] * 6,
+        out_specs=(in_hbm,) * 6,
+        scratch_shapes=[sem((6,))],
         compiler_params=pltpu.CompilerParams(vmem_limit_bytes=16 << 20),
     )(*rows_of)
     heads = (BATCH, 1, TOK, DK)
-    return tuple(out.reshape(heads) for out in outs[:4]) + tuple(outs[4:])
+    return tuple(out.reshape(heads) for out in outs[:4]) + (outs[4].reshape(BATCH, TOK, DV), outs[5])
 
 
 def solution(mesh):

time: 43.4 us -> 43.3 us (level)
  no operation moved by 1% of the time
where the time goes in v3:
time: 43.3 us; the launch traced here: 43.1 us
  Pallas kernels  42.4 us (98%)
  between operations  0.64 us (1%)
    pallas_call x1, Pallas kernels, per_device(): pl.pallas_call(kernel, out_shape=(shape(narrow, BF16), shape(narrow, BF16...  41.2 us
    pallas_call x1, Pallas kernels, per_device(): pl.pallas_call(finish, out_shape=(shape(narrow, BF16), shape(narrow, BF16...  1.28 us

profile of v3, /device:TPU:1, one launch (start us, length us, event | category | flops | bytes accessed | tf_op | source)
XLA Modules:
  0.0 43.1 jit_solution(5319910077838156583)
XLA Ops:
  0.6 41.2 %shard_map.118 = (bf16[16,64,64]{2,1,0:T(8,128)(2,1)S(1)}, bf16[16,64,64]{2,1,0:T(8,128)(2,1)S(1)}, f32[16,64,64]{2,1,0:T(8,128)S(1)}, f32[16,64,64]{2,1,0:T(8,1...) custom-call(bf16[16,64,1024]{2,1,0:T(8,128)(2,1)} %hidden.1, bf16[1024,128]{1,0:T(8,128)(2,1)} %weight.1, ...), custom_call_target="tpu_custom_call" | custom-call | tf_op jit(solution)/shard_map/pallas_call | solution.py:481
  41.8 1.3 %shard_map.119 = (bf16[16,64,64]{2,1,0:T(8,128)(2,1)}, bf16[16,64,64]{2,1,0:T(8,128)(2,1)}, f32[16,64,64]{2,1,0:T(8,128)}, f32[16,64,64]{2,1,0:T(8,128)}, bf16[1024,128]{1,0:T(8,128)(2,1)}, /*index=5*/f32[64,128]{1,0:T(8,128)}) custom-call(bf16[16,64,64]{2,1,0:T(8,128)(2,1)S(1)} %get-tuple-element.18.refs_0_, ...), custom_call_target="tpu_custom_call" | custom-call | tf_op jit(solution)/shard_map/pallas_call | solution.py:540

commit v4 on v3

--- a/solution.py
+++ b/solution.py
@@ -231,7 +231,6 @@
         w_copy(r).start()
         return carry
 
-    lax.fori_loop(1, TP, w_send, 0)
     own_w = pltpu.make_async_copy(
         w.at[pl.ds(pl.multiple_of(tp * DV, DV), DV)],
         wx.at[pl.ds(pl.multiple_of(tp * DV, DV), DV)],
@@ -244,6 +243,7 @@
         rows = hid[pl.ds(b * 4, 4)].reshape(BLK, WIDTH)
         sends[VV, pl.ds(b * BLK, BLK)] = dot(rows, w[...]).astype(BF16)
     send_all(VV)
+    lax.fori_loop(1, TP, w_send, 0)
 
     def turn(t, carry):
         at = pl.ds(pl.multiple_of(t * 128, 128), 128)
@@ -396,14 +396,12 @@
     own_w.wait()
 
     def term(chip, cc):
-        total = None
-        for c in range(2):
-            head = chip * 2 + c
+        rows, cols = [], []
+        for head in (chip * 2, chip * 2 + 1):
             row = head * ROWS + ((z + 4 - cc) % 4) * BLK
-            rows = dall[pl.ds(pl.multiple_of(row, BLK), BLK)]
-            part = dot_nt(rows, wx[pl.ds(pl.multiple_of(head * DV, DV), DV)])
-            total = part if total is None else total + part
-        return total
+            rows.append(dall[pl.ds(pl.multiple_of(row, BLK), BLK)])
+            cols.append(wx[pl.ds(pl.multiple_of(head * DV, DV), DV)])
+        return dot_nt(jnp.concatenate(rows, axis=1), jnp.concatenate(cols, axis=1))
 
     for cc in range(4):
         head_l, head_r = left * 2 + core, right * 2 + core

time: 43.3 us -> 43.3 us (level)
  no operation moved by 1% of the time
where the time goes in v4:
time: 43.3 us; the launch traced here: 43.2 us
  Pallas kernels  42.6 us (98%)
  between operations  0.64 us (1%)
    pallas_call x1, Pallas kernels, per_device(): pl.pallas_call(kernel, out_shape=(shape(narrow, BF16), shape(narrow, BF16...  41.3 us
    pallas_call x1, Pallas kernels, per_device(): pl.pallas_call(finish, out_shape=(shape(narrow, BF16), shape(narrow, BF16...  1.28 us

profile of v4, /device:TPU:1, one launch (start us, length us, event | category | flops | bytes accessed | tf_op | source)
XLA Modules:
  0.0 43.2 jit_solution(11607074244000521535)
XLA Ops:
  0.6 41.3 %shard_map.118 = (bf16[16,64,64]{2,1,0:T(8,128)(2,1)S(1)}, bf16[16,64,64]{2,1,0:T(8,128)(2,1)S(1)}, f32[16,64,64]{2,1,0:T(8,128)S(1)}, f32[16,64,64]{2,1,0:T(8,1...) custom-call(bf16[16,64,1024]{2,1,0:T(8,128)(2,1)} %hidden.1, bf16[1024,128]{1,0:T(8,128)(2,1)} %weight.1, ...), custom_call_target="tpu_custom_call" | custom-call | tf_op jit(solution)/shard_map/pallas_call | solution.py:479
  41.9 1.3 %shard_map.119 = (bf16[16,64,64]{2,1,0:T(8,128)(2,1)}, bf16[16,64,64]{2,1,0:T(8,128)(2,1)}, f32[16,64,64]{2,1,0:T(8,128)}, f32[16,64,64]{2,1,0:T(8,128)}, bf16[1024,128]{1,0:T(8,128)(2,1)}, /*index=5*/f32[64,128]{1,0:T(8,128)}) custom-call(bf16[16,64,64]{2,1,0:T(8,128)(2,1)S(1)} %get-tuple-element.18.refs_0_, ...), custom_call_target="tpu_custom_call" | custom-call | tf_op jit(solution)/shard_map/pallas_call | solution.py:538

commit v5 on v3

--- a/solution.py
+++ b/solution.py
@@ -14,6 +14,8 @@
 ROWS = BATCH * TOK
 BLK = 256
 NBLK = ROWS // BLK
+FAR_FIRST = (10, 6, 9, 14, 11, 5, 15, 13, 7, 2, 8, 1, 4, 3, 12)
+NEAR_FIRST = FAR_FIRST[::-1]
 STEP = 2.0**-16
 QK, DEC, DO, VV, DVT, DQK, GG, GW = range(8)
 
@@ -129,7 +131,7 @@
         load.start()
 
     def peer_of(r):
-        m = (r * 7) % SP
+        m = r
         return ((z + m // 4) % 4) * 4 + (y + m % 4) % 4
 
     def landing(kind, frm):
@@ -163,11 +165,8 @@
         )
 
     def send_all(kind):
-        def body(r, carry):
-            sp_copy(kind, r, peer_of(r)).start()
-            return carry
-
-        lax.fori_loop(1, SP, body, 0)
+        for m in NEAR_FIRST if kind == VV else FAR_FIRST:
+            sp_copy(kind, m, peer_of(m)).start()
         own_copy(kind).start()
 
     def wait_all(kind):

time: 43.3 us -> 43.1 us (level)
  no operation moved by 1% of the time
where the time goes in v5:
time: 43.1 us; the launch traced here: 43 us
  Pallas kernels  42.3 us (98%)
  between operations  0.64 us (1%)
    pallas_call x1, Pallas kernels, per_device(): pl.pallas_call(kernel, out_shape=(shape(narrow, BF16), shape(narrow, BF16...  41 us
    pallas_call x1, Pallas kernels, per_device(): pl.pallas_call(finish, out_shape=(shape(narrow, BF16), shape(narrow, BF16...  1.28 us

profile of v5, /device:TPU:1, one launch (start us, length us, event | category | flops | bytes accessed | tf_op | source)
XLA Modules:
  0.0 43.0 jit_solution(8510494979777314433)
XLA Ops:
  0.6 41.0 %shard_map.118 = (bf16[16,64,64]{2,1,0:T(8,128)(2,1)S(1)}, bf16[16,64,64]{2,1,0:T(8,128)(2,1)S(1)}, f32[16,64,64]{2,1,0:T(8,128)S(1)}, f32[16,64,64]{2,1,0:T(8,1...) custom-call(bf16[16,64,1024]{2,1,0:T(8,128)(2,1)} %hidden.1, bf16[1024,128]{1,0:T(8,128)(2,1)} %weight.1, ...), custom_call_target="tpu_custom_call" | custom-call | tf_op jit(solution)/shard_map/pallas_call | solution.py:480
  41.7 1.3 %shard_map.119 = (bf16[16,64,64]{2,1,0:T(8,128)(2,1)}, bf16[16,64,64]{2,1,0:T(8,128)(2,1)}, f32[16,64,64]{2,1,0:T(8,128)}, f32[16,64,64]{2,1,0:T(8,128)}, bf16[1024,128]{1,0:T(8,128)(2,1)}, /*index=5*/f32[64,128]{1,0:T(8,128)}) custom-call(bf16[16,64,64]{2,1,0:T(8,128)(2,1)S(1)} %get-tuple-element.18.refs_0_, ...), custom_call_target="tpu_custom_call" | custom-call | tf_op jit(solution)/shard_map/pallas_call | solution.py:539

commit v6 on v5

--- a/solution.py
+++ b/solution.py
@@ -407,11 +407,11 @@
     for cc in range(4):
         head_l, head_r = left * 2 + core, right * 2 + core
         to_chip(head_l, cc, 0, left).wait_recv()
-        if cc % 2 == 0:
+        if cc < 2:
             to_chip(head_l, cc, 2, right).start()
         to_core(head_l, cc, 1).start()
         to_chip(head_r, cc, 1, right).wait_recv()
-        if cc % 2 == 1:
+        if cc >= 2:
             to_chip(head_r, cc, 2, left).start()
         to_core(head_r, cc, 2).start()
     for cc in range(4):

time: 43.1 us -> 43.1 us (level)
  no operation moved by 1% of the time
where the time goes in v6:
time: 43.1 us; the launch traced here: 43 us
  Pallas kernels  42.3 us (98%)
  between operations  0.64 us (1%)
    pallas_call x1, Pallas kernels, per_device(): pl.pallas_call(kernel, out_shape=(shape(narrow, BF16), shape(narrow, BF16...  41 us
    pallas_call x1, Pallas kernels, per_device(): pl.pallas_call(finish, out_shape=(shape(narrow, BF16), shape(narrow, BF16...  1.28 us

profile of v6, /device:TPU:1, one launch (start us, length us, event | category | flops | bytes accessed | tf_op | source)
XLA Modules:
  0.0 43.0 jit_solution(960808473723856611)
XLA Ops:
  0.6 41.0 %shard_map.118 = (bf16[16,64,64]{2,1,0:T(8,128)(2,1)S(1)}, bf16[16,64,64]{2,1,0:T(8,128)(2,1)S(1)}, f32[16,64,64]{2,1,0:T(8,128)S(1)}, f32[16,64,64]{2,1,0:T(8,1...) custom-call(bf16[16,64,1024]{2,1,0:T(8,128)(2,1)} %hidden.1, bf16[1024,128]{1,0:T(8,128)(2,1)} %weight.1, ...), custom_call_target="tpu_custom_call" | custom-call | tf_op jit(solution)/shard_map/pallas_call | solution.py:480
  41.7 1.3 %shard_map.119 = (bf16[16,64,64]{2,1,0:T(8,128)(2,1)}, bf16[16,64,64]{2,1,0:T(8,128)(2,1)}, f32[16,64,64]{2,1,0:T(8,128)}, f32[16,64,64]{2,1,0:T(8,128)}, bf16[1024,128]{1,0:T(8,128)(2,1)}, /*index=5*/f32[64,128]{1,0:T(8,128)}) custom-call(bf16[16,64,64]{2,1,0:T(8,128)(2,1)S(1)} %get-tuple-element.18.refs_0_, ...), custom_call_target="tpu_custom_call" | custom-call | tf_op jit(solution)/shard_map/pallas_call | solution.py:539
